TPU v7x, 32 devices: a whole 2x2x4 slice. The times are simulated.
32 devices in a mesh: ep: 8 (over z, y), tp: 4 (over x, core).
Axes of the slice: x: 2, y: 2, z: 4, core: 2. Of those that a mesh axis runs over, the one named last changes fastest.
Arguments:
- queries: bfloat16 [8192, 1024], P('ep', 'tp'), may hold values from -6 to 6
- key_rows: bfloat16 [8192, 256], P('ep', 'tp'), may hold values from -6 to 6
- values: bfloat16 [8192, 256], P('ep', 'tp'), may hold values from -6 to 6
- sink_logit: float32 [16], P('tp'), may hold values from 3 to 7
- out_weight: bfloat16 [1024, 2048], P('tp'), may hold values from -0.1875 to 0.1875
- out_gain: float32 [2048], replicated, may hold values from 0.1 to 1.9
- routed_tokens: bfloat16 [16384, 2048], P(('ep', 'tp')), may hold values from -6 to 6
- expert_ids: int32 [16384, 2], P(('ep', 'tp')), may hold values from 0 to 31, as said below
- route_weight: float32 [16384, 2], P(('ep', 'tp')), may hold values from 0.1 to 1
- routed_gain: float32 [2048], replicated, may hold values from 0.1 to 1.9
- expert_gate: bfloat16 [32, 2048, 1024], P('ep', None, 'tp'), may hold values from -0.125 to 0.125
- expert_up: bfloat16 [32, 2048, 1024], P('ep', None, 'tp'), may hold values from -0.125 to 0.125
- expert_down: bfloat16 [32, 2048, 1024], P('ep', None, 'tp'), may hold values from -0.1875 to 0.1875
Outputs:
- mixer_out: bfloat16 [8192, 2048], P(('ep', 'tp'))
- experts_out: bfloat16 [16384, 2048], P(('ep', 'tp'))
Inputs may be any that keep to these rules, and one draw needn't show every extreme that they name: `expert_ids`: both experts of a row lie in one group (equal id // 8); the 512 rows of one device name every group exactly 512 / 4 times; the rows of one device name no expert more than 64 times; in every device's rows some expert of each group is named exactly 64 times, and one expert is named exactly 64 times by the rows of every device.
All inputs are finite; a program needn't handle non-finite values.
Results may differ from a plain program's by a relative error of at most 0.0071.
Values may be sent and summed in bfloat16 or wider, within the bound.
A program may use at most 192 MiB of HBM per device.

v0:
```python
import jax
import jax.numpy as jnp
from jax import lax
from jax.sharding import PartitionSpec as P

HEAD_DIM = 64
WINDOW = 128
QBLOCK = 512
EXPERTS = 32
TOP = 2
CAP = 64
epsilon = 1e-06


def padded(block, sides, width):
    for axis, dim in sides:
        count = lax.axis_size(axis)
        forward = [(i, i + 1) for i in range(count - 1)]
        backward = [(target, source) for source, target in forward]
        low = lax.ppermute(
            lax.slice_in_dim(block, block.shape[dim] - width, None, axis=dim), axis, forward
        )
        high = lax.ppermute(lax.slice_in_dim(block, 0, width, axis=dim), axis, backward)
        block = jnp.concatenate([low, block, high], axis=dim)
    return block


def local(
    queries,
    key_rows,
    values,
    sink_logit,
    out_weight,
    out_gain,
    routed_tokens,
    expert_ids,
    route_weight,
    routed_gain,
    expert_gate,
    expert_up,
    expert_down,
):
    row_count = queries.shape[0]
    heads_here = queries.shape[1] // HEAD_DIM
    kv_here = key_rows.shape[1] // HEAD_DIM
    group_size = heads_here // kv_here
    width = out_weight.shape[1]
    paired = jnp.concatenate((key_rows, values), axis=1)
    extended = padded(paired, (("ep", 0),), WINDOW)
    offset = lax.axis_index("ep") * row_count
    seq_total = row_count * lax.axis_size("ep")
    grouped = queries.reshape(row_count, kv_here, group_size, HEAD_DIM)
    sinks = sink_logit.reshape(kv_here, group_size)[:, :, None, None]
    span_keys = QBLOCK + 2 * WINDOW

    def attend_block(block_index):
        start_row = block_index * QBLOCK
        query_block = lax.dynamic_slice_in_dim(grouped, start_row, QBLOCK, 0)
        band = lax.dynamic_slice_in_dim(extended, start_row, span_keys, 0)
        key_block = band[:, : kv_here * HEAD_DIM].reshape(span_keys, kv_here, HEAD_DIM)
        value_block = band[:, kv_here * HEAD_DIM :].reshape(span_keys, kv_here, HEAD_DIM)
        scores = jnp.einsum(
            "qhgd,khd->hgqk", query_block, key_block, preferred_element_type=jnp.float32
        ) * HEAD_DIM ** (-0.5)
        query_pos = offset + start_row + jnp.arange(QBLOCK, dtype=jnp.int32)
        key_pos = offset + start_row - WINDOW + jnp.arange(span_keys, dtype=jnp.int32)
        valid = (
            (jnp.abs(key_pos[None, :] - query_pos[:, None]) <= WINDOW)
            & (key_pos[None, :] >= 0)
            & (key_pos[None, :] < seq_total)
        )
        masked = jnp.where(valid, scores, -1e30)
        largest = jnp.maximum(jnp.max(masked, axis=-1, keepdims=True), sinks)
        raised = jnp.where(valid, jnp.exp(masked - largest), 0.0)
        denominator = jnp.sum(raised, axis=-1, keepdims=True) + jnp.exp(sinks - largest)
        weights = (raised / denominator).astype(jnp.bfloat16)
        attended = jnp.einsum(
            "hgqk,khd->qhgd", weights, value_block, preferred_element_type=jnp.float32
        )
        return attended.astype(jnp.bfloat16).reshape(QBLOCK, heads_here * HEAD_DIM)

    attended = lax.map(attend_block, jnp.arange(row_count // QBLOCK, dtype=jnp.int32))
    attended = attended.reshape(row_count, heads_here * HEAD_DIM)
    mixed = lax.psum_scatter(
        jnp.dot(attended, out_weight, preferred_element_type=jnp.float32),
        "tp",
        scatter_dimension=0,
        tiled=True,
    )
    mixer_out = (
        mixed * lax.rsqrt(jnp.mean(mixed * mixed, axis=-1, keepdims=True) + epsilon) * out_gain
    ).astype(jnp.bfloat16)
    token_total = routed_tokens.shape[0]
    inputs = routed_tokens.astype(jnp.float32)
    normed = (
        inputs
        * lax.rsqrt(jnp.mean(inputs * inputs, axis=-1, keepdims=True) + epsilon)
        * routed_gain
    ).astype(jnp.bfloat16)
    flat_ids = expert_ids.reshape(-1)
    onehot = (flat_ids[:, None] == jnp.arange(EXPERTS, dtype=jnp.int32)[None, :]).astype(jnp.int32)
    earlier = jnp.cumsum(onehot, axis=0) - onehot
    slot_index = jnp.sum(earlier * onehot, axis=1)
    flat_dest = slot_index * EXPERTS + flat_ids
    source_rows = jnp.arange(token_total * TOP, dtype=jnp.int32) // TOP
    slot_token = jnp.full((CAP * EXPERTS,), token_total, jnp.int32).at[flat_dest].set(source_rows)
    outgoing = jnp.take(normed, slot_token, axis=0, mode="fill", fill_value=0).reshape(
        1, CAP, EXPERTS, width
    )
    arrived = lax.all_to_all(outgoing, "ep", split_axis=2, concat_axis=0, tiled=True)
    source_count, slot_count, local_experts, feature_count = arrived.shape
    rows_in = arrived.reshape(source_count * slot_count, local_experts, feature_count)
    gate_piece = lax.all_gather(expert_gate, "tp", axis=2, tiled=True)
    up_piece = lax.all_gather(expert_up, "tp", axis=2, tiled=True)
    down_piece = lax.all_gather(expert_down, "tp", axis=2, tiled=True)
    gate = jnp.einsum("red,edf->ref", rows_in, gate_piece, preferred_element_type=jnp.float32)
    upward = jnp.einsum("red,edf->ref", rows_in, up_piece, preferred_element_type=jnp.float32)
    hidden = (jax.nn.silu(gate) * upward).astype(jnp.bfloat16)
    summed = jnp.einsum("ref,edf->red", hidden, down_piece, preferred_element_type=jnp.float32)
    produced = summed.astype(jnp.bfloat16).reshape(
        source_count, slot_count, local_experts, feature_count
    )
    returned = lax.all_to_all(produced, "ep", split_axis=0, concat_axis=2, tiled=True)
    returned = returned.reshape(CAP * EXPERTS, width)
    picked_rows = jnp.take(returned, flat_dest, axis=0).reshape(token_total, TOP, width)
    experts_out = jnp.sum(
        picked_rows.astype(jnp.float32) * route_weight[:, :, None], axis=1
    ).astype(jnp.bfloat16)
    return (mixer_out, experts_out)


def solution(mesh):
    placed = (
        P("ep", "tp"),
        P("ep", "tp"),
        P("ep", "tp"),
        P("tp"),
        P("tp", None),
        P(),
        P(("ep", "tp"), None),
        P(("ep", "tp"), None),
        P(("ep", "tp"), None),
        P(),
        P("ep", None, "tp"),
        P("ep", None, "tp"),
        P("ep", None, "tp"),
    )
    return jax.shard_map(
        local,
        mesh=mesh,
        in_specs=placed,
        out_specs=(P(("ep", "tp"), None), P(("ep", "tp"), None)),
        check_vma=False,
    )
```

profile of v0, /device:TPU:0, one launch (start us, length us, event | category | flops | bytes accessed | tf_op | source)
XLA Modules:
  0.0 638.6 jit_solution(18265312052773669787)
XLA Ops:
  10.1 9.0 %reduce-window.6 = s32[32,8,128]{2,1,0:T(8,128)S(1)} reduce-window(s32[32,8,128]{2,1,0:T(8,128)S(1)} %fusion.28, s32[]{:T(128)} %constant.129.clone.1), window={size=1x1x128 pad=0_0x0_0x127_0}, to_apply=%region_6.7 | reduce-window | flops 4161536 | bytes 262148 | tf_op jit(solution)/shard_map/reduce-window
  20.3 4.3 scatter_custom_fusion
  27.9 11.0 %gather_fusion = bf16[2048,2048]{1,0:T(8,128)(2,1)} fusion(bf16[512,2048]{1,0:T(8,128)(2,1)S(1)} %fusion.24, s32[2048]{0:T(1024)S(1)} %fusion.29), kind=kCustom, calls=%fused_computation | custom fusion | bytes 16785408 | tf_op jit(solution)/shard_map/jit(_take)/gather | solution.py:107
  39.0 16.8 %copy_select_fusion = bf16[1,64,32,2048]{3,1,0,2:T(8,128)(2,1)} fusion(bf16[1,64,32,2048]{3,2,1,0:T(8,128)(2,1)} %bitcast.124, pred[64,32]{0,1:T(8,128)(4,1)S(1)} %copy.59), kind=kLoop, calls=%fused_computation.37 | loop fusion | flops 4194304 | bytes 16779264 | tf_op jit(solution)/shard_map/jit(_take)/select_n | solution.py:107
  55.7 7.2 %all-to-all-start = ((bf16[1,64,32,2048]{3,1,0,2:T(8,128)(2,1)}), bf16[1,64,32,2048]{3,1,0,2:T(8,128)(2,1)}, u32[]{:S(2)}, u32[]{:S(2)}) async-start(bf16[1,64,32,2048]{3,1,0,2:T(8,128)(2,1)} %copy_select_fusion), calls=%async_computation.1 | async-start | bytes 16777216 | tf_op jit(solution)/shard_map/all_to_all | solution.py:110
  69.7 62.0 %collective-permute-done = bf16[128,128]{0,1:T(8,128)(2,1)S(1)} collective-permute-done((bf16[128,128]{0,1:T(8,128)(2,1)S(1)}, bf16[128,128]{0,1:T(8,128)(2,1)S(1)}, u32[]{:S(2)}, u32[]{:S(2)}) %collective-permute-start) | collective-permute-done | bytes 32800 | tf_op jit(solution)/shard_map/ppermute | solution.py:20
  131.8 26.2 %while.12 = (s32[]{:T(128)}, bf16[2,512,256]{2,1,0:T(8,128)(2,1)S(1)}, s32[2]{0:T(128)S(1)}, bf16[1280,128]{0,1:T(8,128)(2,1)S(1)}, s32[]{:T(128)}, /*index=5*/b...) while((s32[]{:T(128)}, ...), condition=%wide.region_3.4_spmd, body=%wide.region_0.3_spmd.sunk | while | flops 426778112 | bytes 47478104 | solution.py:82
  140.0 5.0 fusion.57
  152.8 5.0 fusion.57
  158.1 4.5 fusion.37
  162.6 83.9 %all-to-all-done = bf16[1,64,32,2048]{3,1,0,2:T(8,128)(2,1)} async-done(((bf16[1,64,32,2048]{3,1,0,2:T(8,128)(2,1)}), bf16[1,64,32,2048]{3,1,0,2:T(8,128)(2,1)}, u32[]{:S(2)}, u32[]{:S(2)}) %all-to-all-start) | async-done | bytes 8388640 | tf_op jit(solution)/shard_map/all_to_all | solution.py:110
  246.5 8.9 %copy.61 = bf16[8,1,64,4,2048]{4,2,0,3,1:T(8,128)(2,1)} copy(bf16[8,1,64,4,2048]{4,2,3,0,1:T(8,128)(2,1)} %bitcast.20) | data formatting | bytes 16777216 | tf_op jit(solution)/shard_map/all_to_all | solution.py:110
  255.4 17.1 %fusion.38 = f32[4,512,1024]{2,1,0:T(8,128)} fusion(bf16[512,4,2048]{2,0,1:T(8,128)(2,1)} %bitcast.125, bf16[4,2048,1024]{2,1,0:T(8,128)(2,1)} %all-gather.6.cloned.1.call-done), kind=kOutput, calls=%fused_computation.81 | convolution fusion | flops 8589934592 | bytes 33554432 | tf_op jit(solution)/shard_map/red,edf->ref/dot_general | solution.py:117
  272.5 67.5 %all-gather.8.cloned.1.call-done = bf16[4,2048,1024]{2,1,0:T(8,128)(2,1)} async-done(((bf16[4,2048,256]{2,1,0:T(8,128)(2,1)}), bf16[4,2048,1024]{2,1,0:T(8,128)(2,1)}) %all-gather.8.cloned.1.call-update) | async-done | bytes 16777232 | tf_op jit(solution)/shard_map/all_gather | solution.py:115
  340.0 28.9 %convolution_convert_fusion = bf16[4,512,2048]{2,1,0:T(8,128)(2,1)} fusion(bf16[4,2048,1024]{2,1,0:T(8,128)(2,1)} %all-gather.8.cloned.1.call-done, f32[4,512,1024]{2,1,0:T(8,128)} %fusion.38, bf16[512,4,2048]{2,0,1:T(8,128)(2,1)} %bitcast.126, bf16[4,2048,1024]{2,1,0:T(8,128)(2,1)} %all-gather.4.cloned.1.call-done), kind=kOutput, calls=%fused_computation.40 | convolution fusion | flops 17196646400 | bytes 58720256 | tf_op jit(solution)/shard_map/ref,edf->red/dot_general | solution.py:119
  368.9 8.3 %copy.62 = bf16[8,64,4,2048]{3,1,2,0:T(8,128)(2,1)} copy(bf16[8,64,4,2048]{3,1,0,2:T(8,128)(2,1)} %bitcast.127) | data formatting | bytes 16777216 | tf_op jit(solution)/shard_map/reshape | solution.py:120
  377.2 5.7 all-to-all-start.1
  383.6 30.2 %reduce-scatter.2.cloned.1.call-done = f32[256,2048]{1,0:T(8,128)} async-done(((f32[1024,2048]{1,0:T(8,128)}), f32[256,2048]{1,0:T(8,128)}) %reduce-scatter.2.cloned.1.call-update) | async-done | bytes 2097168 | tf_op jit(solution)/shard_map/reduce_scatter | solution.py:84
  418.5 147.9 %all-to-all-done.1 = bf16[8,64,4,2048]{3,1,2,0:T(8,128)(2,1)} async-done(((bf16[8,64,4,2048]{3,1,2,0:T(8,128)(2,1)}), bf16[8,64,4,2048]{3,1,2,0:T(8,128)(2,1)}, u32[]{:S(2)}, u32[]{:S(2)}) %all-to-all-start.1) | async-done | bytes 8388640 | tf_op jit(solution)/shard_map/all_to_all | solution.py:123
  566.4 12.1 %copy.63 = bf16[1,64,8,4,2048]{4,3,2,1,0:T(4,128)(2,1)} copy(bf16[1,64,8,4,2048]{4,1,3,2,0:T(8,128)(2,1)} %bitcast.27) | data formatting | bytes 16777216 | tf_op jit(solution)/shard_map/all_to_all | solution.py:123
  578.5 12.5 %reshape.271 = bf16[2048,2048]{1,0:T(8,128)(2,1)} reshape(bf16[1,64,8,4,2048]{4,3,2,1,0:T(4,128)(2,1)} %copy.63) | data formatting | bytes 16777216 | tf_op jit(solution)/shard_map/reshape | solution.py:124
  591.0 13.4 %gather_fusion.1 = bf16[1024,2048]{1,0:T(8,128)(2,1)} fusion(bf16[2048,2048]{1,0:T(8,128)(2,1)} %reshape.271, s32[1024]{0:T(1024)S(1)} %broadcast_clamp_fusion), kind=kCustom, calls=%fused_computation.1 | custom fusion | bytes 8392704 | tf_op jit(solution)/shard_map/jit(_take)/gather | solution.py:125
  604.4 7.6 %gather.15 = bf16[512,2,2048]{2,1,0:T(2,128)(2,1)} reshape(bf16[1024,2048]{1,0:T(8,128)(2,1)} %gather_fusion.1) | data formatting | bytes 8388608 | tf_op jit(solution)/shard_map/jit(_take)/gather | solution.py:125
  612.0 20.0 %multiply_reduce_fusion = bf16[512,2048]{1,0:T(8,128)(2,1)} fusion(bf16[512,2,2048]{2,1,0:T(2,128)(2,1)} %gather.15, pred[512,2]{1,0:T(8,128)(4,1)S(1)} %copy.57, f32[512,2]{1,0:T(8,128)S(1)} %copy.64), kind=kLoop, calls=%fused_computation.38 | loop fusion | flops 7340032 | bytes 6296576 | tf_op jit(solution)/shard_map/reduce_sum | solution.py:126
  (107 shorter events, 34.0 us)
Async XLA Ops:
  7.2 150.9 %copy-start = (bf16[256,2048]{1,0:T(8,128)(2,1)S(1)}, bf16[256,2048]{1,0:T(8,128)(2,1)}, u32[]{:S(2)}) copy-start(bf16[256,2048]{1,0:T(8,128)(2,1)} %param.19) | copy-start | bytes 3145732
  7.2 2.3 copy-start.9
  7.2 248.2 %all-gather.6.cloned.1.call-start = ((), (), s32[]{:S(2)}) async-start(), calls=%async_computation.5 | async-start | bytes 20971520 | tf_op jit(solution)/shard_map/all_gather | solution.py:114
  7.9 16.9 %copy-start.3 = (bf16[512,2048]{1,0:T(8,128)(2,1)S(1)}, bf16[512,2048]{1,0:T(8,128)(2,1)}, u32[]{:S(2)}) copy-start(bf16[512,2048]{1,0:T(8,128)(2,1)} %param.21) | copy-start | bytes 6291460
  7.9 17.4 %copy-start.13 = (f32[2048]{0:T(1024)S(1)}, f32[2048]{0:T(1024)}, u32[]{:S(2)}) copy-start(f32[2048]{0:T(1024)} %param.24) | copy-start | bytes 24580
  7.9 264.5 %all-gather.4.cloned.1.call-start = ((), (), s32[]{:S(2)}) async-start(), calls=%async_computation.4 | async-start | bytes 20971520 | tf_op jit(solution)/shard_map/all_gather | solution.py:113
  8.7 331.3 %all-gather.8.cloned.1.call-start = ((), (), s32[]{:S(2)}) async-start(), calls=%async_computation.6 | async-start | bytes 20971520 | tf_op jit(solution)/shard_map/all_gather | solution.py:115
  20.3 4.3 copy-start.11
  55.7 7.3 %copy-start.4 = (bf16[1024,64]{0,1:T(8,128)(2,1)S(1)}, bf16[1024,64]{0,1:T(8,128)(2,1)}, u32[]{:S(2)}) copy-start(bf16[1024,64]{0,1:T(8,128)(2,1)} %param.16) | copy-start | bytes 393220
  55.7 7.3 %copy-start.5 = (bf16[1024,64]{0,1:T(8,128)(2,1)S(1)}, bf16[1024,64]{0,1:T(8,128)(2,1)}, u32[]{:S(2)}) copy-start(bf16[1024,64]{0,1:T(8,128)(2,1)} %param.17) | copy-start | bytes 393220
  55.7 76.1 %copy-start.6 = (f32[4]{0:T(128)S(1)}, f32[4]{0:T(128)}, u32[]{:S(2)}) copy-start(f32[4]{0:T(128)} %param.18) | copy-start | bytes 52
  55.7 190.7 %all-to-all-start = ((bf16[1,64,32,2048]{3,1,0,2:T(8,128)(2,1)}), bf16[1,64,32,2048]{3,1,0,2:T(8,128)(2,1)}, u32[]{:S(2)}, u32[]{:S(2)}) async-start(bf16[1,64,32,2048]{3,1,0,2:T(8,128)(2,1)} %copy_select_fusion), calls=%async_computation.1 | async-start | bytes 16777216 | tf_op jit(solution)/shard_map/all_to_all | solution.py:110
  63.0 350.9 %reduce-scatter.2.cloned.1.call-start = ((), (), s32[]{:S(2)}) async-start(), calls=%async_computation.3 | async-start | bytes 10485760 | tf_op jit(solution)/shard_map/reduce_scatter | solution.py:84
  63.1 68.7 %collective-permute-start = (bf16[128,128]{0,1:T(8,128)(2,1)S(1)}, bf16[128,128]{0,1:T(8,128)(2,1)S(1)}, u32[]{:S(2)}, u32[]{:S(2)}) collective-permute-start(bf16[128,128]{0,1:T(8,128)(2,1)S(1)} %get-tuple-element.110), channel_id=1, source_target_pairs={{0,4},{4,8},{8,12},{12,16},{16,20},{20,24},{24,28},{1,5},{5,9},{9,... | collective-permute-start | bytes 98312 | tf_op jit(solution)/shard_map/ppermute | solution.py:20
  67.0 64.8 %collective-permute-start.1 = (bf16[128,128]{0,1:T(8,128)(2,1)S(1)}, bf16[128,128]{0,1:T(8,128)(2,1)S(1)}, u32[]{:S(2)}, u32[]{:S(2)}) collective-permute-start(bf16[128,128]{0,1:T(8,128)(2,1)S(1)} %get-tuple-element.111), channel_id=1, source_target_pairs={{4,0},{8,4},{12,8},{16,12},{20,16},{24,20},{28,24},{5,1},{9,5},{13... | collective-permute-start | bytes 98312 | tf_op jit(solution)/shard_map/ppermute | solution.py:23
  135.1 3.2 copy-start.2
  148.5 2.7 copy-start.2
  377.1 5.8 copy-start.8
  377.1 6.1 copy-start.10
  377.1 6.3 copy-start.15
  377.1 6.5 %copy-start.12 = (s32[1024,1]{0,1:T(1,128)S(1)}, s32[1024,1]{0,1:T(1,128)}, u32[]{:S(2)}) copy-start(s32[1024,1]{0,1:T(1,128)} %copy-done.11) | copy-start | bytes 12292
  377.1 38.5 %copy-start.14 = (f32[2048]{0:T(1024)S(1)}, f32[2048]{0:T(1024)}, u32[]{:S(2)}) copy-start(f32[2048]{0:T(1024)} %param.20) | copy-start | bytes 24580
  377.2 189.2 %all-to-all-start.1 = ((bf16[8,64,4,2048]{3,1,2,0:T(8,128)(2,1)}), bf16[8,64,4,2048]{3,1,2,0:T(8,128)(2,1)}, u32[]{:S(2)}, u32[]{:S(2)}) async-start(bf16[8,64,4,2048]{3,1,2,0:T(8,128)(2,1)} %copy.62), calls=%async_computation.2 | async-start | bytes 16777216 | tf_op jit(solution)/shard_map/all_to_all | solution.py:123
  591.0 41.0 %copy-start.1 = (bf16[256,2048]{1,0:T(8,128)(2,1)S(1)}, bf16[256,2048]{1,0:T(8,128)(2,1)}, u32[]{:S(2)}) copy-start(bf16[256,2048]{1,0:T(8,128)(2,1)} %param.19) | copy-start | bytes 3145732
  (1 other events, 0.6 us)
Sparse Core Ops, SparseCore 0:
  9.5 110.8 all-gather.5
  122.0 108.1 all-gather.3
  231.8 108.1 all-gather.7
  342.4 71.4 reduce-scatter.1
where the time goes:
time: 640 us; the launch traced here: 639 us
  waiting for transfers between devices  394 us (62%)
  local copies, waits for them, and re-layouts  89 us (14%)
  matrix products  63 us (10%)
  other arithmetic  58.9 us (9%)
  starting transfers between devices  18.5 us (3%)
  between operations  14.1 us (2%)
    all_to_all x1, waiting for transfers between devices, local(): lax.all_to_all(produced, 'ep', split_axis=0, concat_axis=2, tiled=True)  148 us
    all_to_all x1, waiting for transfers between devices, local(): lax.all_to_all(outgoing, 'ep', split_axis=2, concat_axis=0, tiled=True)  83.9 us
    all_gather x1, waiting for transfers between devices, local(): down_piece = lax.all_gather(expert_down, 'tp', axis=2, tiled=True)  67.5 us
    ppermute x1, waiting for transfers between devices, padded(): lax.ppermute(lax.slice_in_dim(block, block.shape[dim] - width, None, axis...  62 us
    reduce_scatter x1, waiting for transfers between devices, local(): lax.psum_scatter(jnp.dot(attended, out_weight, preferred_element_type=jnp...  30.2 us
    dot_general x1, matrix products, local(): jnp.einsum('ref,edf->red', hidden, down_piece, preferred_element_type=jnp...  28.9 us
    gather x2, local copies, waits for them, and re-layouts, local(): jnp.take(returned, flat_dest, axis=0).reshape(token_total, TOP, width)  21 us
    reduce_sum x1, other arithmetic, local(): jnp.sum(picked_rows.astype(jnp.float32) * route_weight[:, :, None], axis=1)  20 us
  transfers between devices with their start and end apart: 8, of which 5 were waited for; matrix products, arithmetic and copies ran while one was open for 22% of the time, Pallas kernels for 0%

commit v1 on v0

--- a/solution.py
+++ b/solution.py
@@ -112,11 +112,40 @@
     rows_in = arrived.reshape(source_count * slot_count, local_experts, feature_count)
     gate_piece = lax.all_gather(expert_gate, "tp", axis=2, tiled=True)
     up_piece = lax.all_gather(expert_up, "tp", axis=2, tiled=True)
-    down_piece = lax.all_gather(expert_down, "tp", axis=2, tiled=True)
     gate = jnp.einsum("red,edf->ref", rows_in, gate_piece, preferred_element_type=jnp.float32)
     upward = jnp.einsum("red,edf->ref", rows_in, up_piece, preferred_element_type=jnp.float32)
     hidden = (jax.nn.silu(gate) * upward).astype(jnp.bfloat16)
-    summed = jnp.einsum("ref,edf->red", hidden, down_piece, preferred_element_type=jnp.float32)
+    peers, index, width_2 = (lax.axis_size("tp"), lax.axis_index("tp"), expert_down.shape[2])
+    ahead = [(i_2, (i_2 + 1) % peers) for i_2 in range(peers)]
+    left = [(i_2, (i_2 - 1) % peers) for i_2 in range(peers)]
+    halfway = peers // 2
+    from_left = from_right = expert_down
+    summed = jnp.einsum(
+        "ref,edf->red",
+        lax.dynamic_slice_in_dim(hidden, index * width_2, expert_down.shape[2], axis=2),
+        expert_down,
+        preferred_element_type=jnp.float32,
+    )
+    for step in range(1, halfway + 1):
+        from_left = lax.ppermute(from_left, "tp", ahead)
+        if step < peers - halfway:
+            from_right = lax.ppermute(from_right, "tp", left)
+            summed = summed + jnp.einsum(
+                "ref,edf->red",
+                lax.dynamic_slice_in_dim(
+                    hidden, (index + step) % peers * width_2, from_right.shape[2], axis=2
+                ),
+                from_right,
+                preferred_element_type=jnp.float32,
+            )
+        summed = summed + jnp.einsum(
+            "ref,edf->red",
+            lax.dynamic_slice_in_dim(
+                hidden, (index - step) % peers * width_2, from_left.shape[2], axis=2
+            ),
+            from_left,
+            preferred_element_type=jnp.float32,
+        )
     produced = summed.astype(jnp.bfloat16).reshape(
         source_count, slot_count, local_experts, feature_count
     )

time: 640 us -> 678 us (1.059)
  matrix products: 63 us -> 104 us
  waiting for transfers between devices: 394 us -> 385 us
    ppermute x0 -> x3, waiting for transfers between devices: none -> 70.9 us  [the longest x2 70.9 us: local(): from_left = lax.ppermute(from_left, 'tp', ahead)]
    all_to_all x1, waiting for transfers between devices: 83.9 us -> 13.4 us  [local(): lax.all_to_all(outgoing, 'ep', split_axis=2, concat_axis=0, tiled=True)]
    all_gather x1 -> x0, waiting for transfers between devices: 67.5 us -> none  [local(): down_piece = lax.all_gather(expert_down, 'tp', axis=2, tiled=True)]
    all_gather x1, waiting for transfers between devices: 0.01 us -> 59.4 us  [local(): gate_piece = lax.all_gather(expert_gate, 'tp', axis=2, tiled=True)]
    dot_general x1 -> x5, matrix products: 28.9 us -> 70.6 us  [the longest x2 32.9 us: local(): jnp.einsum('ref,edf->red', lax.dynamic_slice_in_dim(hidden, (index - step...]
    all_to_all x1, waiting for transfers between devices: 148 us -> 178 us  [local(): lax.all_to_all(produced, 'ep', split_axis=0, concat_axis=2, tiled=True)]
    reduce_scatter x1, waiting for transfers between devices: 30.2 us -> 0.02 us  [local(): lax.psum_scatter(jnp.dot(attended, out_weight, preferred_element_type=jnp...]
  transfers between devices with their start and end apart: 8 -> 10, of which waited for: 5 -> 5; matrix products, arithmetic and copies ran while one was open for 22% -> 27% of each run, Pallas kernels for 0% -> 0%
where the time goes in v1:
time: 678 us; the launch traced here: 671 us
  waiting for transfers between devices  385 us (57%)
  matrix products  104 us (15%)
  local copies, waits for them, and re-layouts  87.7 us (13%)
  other arithmetic  58.9 us (9%)
  starting transfers between devices  19.5 us (3%)
  between operations  14.4 us (2%)
    all_to_all x1, waiting for transfers between devices, local(): lax.all_to_all(produced, 'ep', split_axis=0, concat_axis=2, tiled=True)  178 us
    ppermute x2, waiting for transfers between devices, local(): from_left = lax.ppermute(from_left, 'tp', ahead)  70.9 us
    ppermute x1, waiting for transfers between devices, padded(): lax.ppermute(lax.slice_in_dim(block, block.shape[dim] - width, None, axis...  61.4 us
    all_gather x1, waiting for transfers between devices, local(): gate_piece = lax.all_gather(expert_gate, 'tp', axis=2, tiled=True)  59.4 us
    dot_general x2, matrix products, local(): jnp.einsum('ref,edf->red', lax.dynamic_slice_in_dim(hidden, (index - step...  32.9 us
    gather x2, local copies, waits for them, and re-layouts, local(): jnp.take(returned, flat_dest, axis=0).reshape(token_total, TOP, width)  21 us
    reduce_sum x1, other arithmetic, local(): jnp.sum(picked_rows.astype(jnp.float32) * route_weight[:, :, None], axis=1)  20 us
    dot_general x1, matrix products, local(): jnp.einsum('red,edf->ref', rows_in, gate_piece, preferred_element_type=jn...  18.6 us
  transfers between devices with their start and end apart: 10, of which 5 were waited for; matrix products, arithmetic and copies ran while one was open for 27% of the time, Pallas kernels for 0%

profile of v1, /device:TPU:0, one launch (start us, length us, event | category | flops | bytes accessed | tf_op | source)
XLA Modules:
  0.0 670.9 jit_solution(5561233337844783146)
XLA Ops:
  9.4 9.0 %reduce-window.6 = s32[32,8,128]{2,1,0:T(8,128)S(1)} reduce-window(s32[32,8,128]{2,1,0:T(8,128)S(1)} %fusion.35, s32[]{:T(128)} %constant.153.clone.1), window={size=1x1x128 pad=0_0x0_0x127_0}, to_apply=%region_6.7 | reduce-window | flops 4161536 | bytes 262148 | tf_op jit(solution)/shard_map/reduce-window
  27.3 11.0 %gather_fusion = bf16[2048,2048]{1,0:T(8,128)(2,1)} fusion(bf16[512,2048]{1,0:T(8,128)(2,1)S(1)} %fusion.24, s32[2048]{0:T(1024)S(1)} %fusion.36), kind=kCustom, calls=%fused_computation | custom fusion | bytes 16785408 | tf_op jit(solution)/shard_map/jit(_take)/gather | solution.py:107
  38.3 16.8 %copy_select_fusion = bf16[1,64,32,2048]{3,1,0,2:T(8,128)(2,1)} fusion(bf16[1,64,32,2048]{3,2,1,0:T(8,128)(2,1)} %bitcast.123, pred[64,32]{0,1:T(8,128)(4,1)S(1)} %copy.59), kind=kLoop, calls=%fused_computation.38 | loop fusion | flops 4194304 | bytes 16779264 | tf_op jit(solution)/shard_map/jit(_take)/select_n | solution.py:107
  55.1 7.3 %all-to-all-start = ((bf16[1,64,32,2048]{3,1,0,2:T(8,128)(2,1)}), bf16[1,64,32,2048]{3,1,0,2:T(8,128)(2,1)}, u32[]{:S(2)}, u32[]{:S(2)}) async-start(bf16[1,64,32,2048]{3,1,0,2:T(8,128)(2,1)} %copy_select_fusion), calls=%async_computation.1 | async-start | bytes 16777216 | tf_op jit(solution)/shard_map/all_to_all | solution.py:110
  69.8 61.4 %collective-permute-done = bf16[128,128]{0,1:T(8,128)(2,1)S(1)} collective-permute-done((bf16[128,128]{0,1:T(8,128)(2,1)S(1)}, bf16[128,128]{0,1:T(8,128)(2,1)S(1)}, u32[]{:S(2)}, u32[]{:S(2)}) %collective-permute-start) | collective-permute-done | bytes 32800 | tf_op jit(solution)/shard_map/ppermute | solution.py:20
  131.2 25.3 %while.12 = (s32[]{:T(128)}, bf16[2,512,256]{2,1,0:T(8,128)(2,1)S(1)}, s32[2]{0:T(128)S(1)}, bf16[1280,128]{0,1:T(8,128)(2,1)S(1)}, s32[]{:T(128)}, /*index=5*/b...) while((s32[]{:T(128)}, ...), condition=%wide.region_3.4_spmd, body=%wide.region_0.3_spmd.sunk | while | flops 426778112 | bytes 47478104 | solution.py:82
  161.1 70.9 %collective-permute-done.3 = bf16[4,2048,256]{2,1,0:T(8,128)(2,1)} collective-permute-done((bf16[4,2048,256]{2,1,0:T(8,128)(2,1)}, bf16[4,2048,256]{2,1,0:T(8,128)(2,1)}, u32[]{:S(2)}, u32[]{:S(2)}) %collective-permute-start.3) | collective-permute-done | bytes 4194336 | tf_op jit(solution)/shard_map/ppermute | solution.py:130
  232.5 13.4 %all-to-all-done = bf16[1,64,32,2048]{3,1,0,2:T(8,128)(2,1)} async-done(((bf16[1,64,32,2048]{3,1,0,2:T(8,128)(2,1)}), bf16[1,64,32,2048]{3,1,0,2:T(8,128)(2,1)}, u32[]{:S(2)}, u32[]{:S(2)}) %all-to-all-start) | async-done | bytes 8388640 | tf_op jit(solution)/shard_map/all_to_all | solution.py:110
  245.9 8.3 %copy.61 = bf16[8,1,64,4,2048]{4,2,0,3,1:T(8,128)(2,1)} copy(bf16[8,1,64,4,2048]{4,2,3,0,1:T(8,128)(2,1)} %bitcast.20) | data formatting | bytes 16777216 | tf_op jit(solution)/shard_map/all_to_all | solution.py:110
  254.2 16.8 %fusion.48 = f32[4,512,1024]{2,1,0:T(8,128)} fusion(bf16[512,4,2048]{2,0,1:T(8,128)(2,1)} %bitcast.125, bf16[4,2048,1024]{2,1,0:T(8,128)(2,1)} %all-gather.5.cloned.1.call-done), kind=kOutput, calls=%fused_computation.91 | convolution fusion | flops 8589934592 | bytes 33554432 | tf_op jit(solution)/shard_map/red,edf->ref/dot_general | solution.py:116
  271.0 59.4 %all-gather.3.cloned.1.call-done = bf16[4,2048,1024]{2,1,0:T(8,128)(2,1)} async-done(((bf16[4,2048,256]{2,1,0:T(8,128)(2,1)}), bf16[4,2048,1024]{2,1,0:T(8,128)(2,1)}) %all-gather.3.cloned.1.call-update) | async-done | bytes 16777232 | tf_op jit(solution)/shard_map/all_gather | solution.py:113
  330.4 18.6 %fusion.18 = bf16[512,4,1024]{2,0,1:T(8,128)(2,1)S(1)} fusion(f32[4,512,1024]{2,1,0:T(8,128)} %fusion.48, bf16[512,4,2048]{2,0,1:T(8,128)(2,1)} %bitcast.126, bf16[4,2048,1024]{2,1,0:T(8,128)(2,1)} %all-gather.3.cloned.1.call-done), kind=kOutput, calls=%fused_computation.32 | convolution fusion | flops 8602517504 | bytes 37748736 | tf_op jit(solution)/shard_map/red,edf->ref/dot_general | solution.py:115
  349.0 8.6 %fusion.30 = f32[4,512,2048]{2,1,0:T(8,128)} fusion(bf16[4,2048,256]{2,1,0:T(8,128)(2,1)S(1)} %copy-done.5, bf16[512,4,1024]{2,0,1:T(8,128)(2,1)S(1)} %fusion.18, s32[]{:T(128)S(6)} %select_n.100), kind=kOutput, calls=%fused_computation.53 | convolution fusion | flops 2147483648 | bytes 22020100 | tf_op jit(solution)/shard_map/ref,edf->red/dot_general | solution.py:123
  357.6 10.4 %fusion.26 = f32[4,512,2048]{2,1,0:T(8,128)} fusion(bf16[4,2048,256]{2,1,0:T(8,128)(2,1)} %collective-permute-done.3, bf16[512,4,1024]{2,0,1:T(8,128)(2,1)S(1)} %fusion.18, s32[]{:T(128)S(6)} %select_n.104), kind=kOutput, calls=%fused_computation.49 | convolution fusion | flops 2147483648 | bytes 22020100 | tf_op jit(solution)/shard_map/ref,edf->red/dot_general | solution.py:141
  368.0 10.4 %fusion.28 = f32[4,512,2048]{2,1,0:T(8,128)} fusion(bf16[4,2048,256]{2,1,0:T(8,128)(2,1)} %collective-permute-done.2, bf16[512,4,1024]{2,0,1:T(8,128)(2,1)S(1)} %fusion.18, s32[]{:T(128)S(6)} %select_n.102), kind=kOutput, calls=%fused_computation.51 | convolution fusion | flops 2147483648 | bytes 22020100 | tf_op jit(solution)/shard_map/ref,edf->red/dot_general | solution.py:133
  378.4 22.5 %add_convert_fusion = bf16[4,512,2048]{2,1,0:T(8,128)(2,1)} fusion(f32[4,512,2048]{2,1,0:T(8,128)} %fusion.26, f32[4,512,2048]{2,1,0:T(8,128)} %fusion.30, f32[4,512,2048]{2,1,0:T(8,128)} %fusion.28, bf16[4,2048,256]{2,1,0:T(8,128)(2,1)} %collective-permute-done.4, bf16[512,4,1024]{2,0,1:T(8,128)(2,1)} %copy-done.4, s32[]{:T(128)S(6)} %select_n.106), kind=kOutput, calls=%fused_computation.30 | convolution fusion | flops 2164260864 | bytes 63963140 | tf_op jit(solution)/shard_map/ref,edf->red/dot_general | solution.py:141
  401.0 8.3 %copy.62 = bf16[8,64,4,2048]{3,1,2,0:T(8,128)(2,1)} copy(bf16[8,64,4,2048]{3,1,0,2:T(8,128)(2,1)} %bitcast.124) | data formatting | bytes 16777216 | tf_op jit(solution)/shard_map/reshape | solution.py:149
  409.3 5.6 all-to-all-start.1
  420.3 178.2 %all-to-all-done.1 = bf16[8,64,4,2048]{3,1,2,0:T(8,128)(2,1)} async-done(((bf16[8,64,4,2048]{3,1,2,0:T(8,128)(2,1)}), bf16[8,64,4,2048]{3,1,2,0:T(8,128)(2,1)}, u32[]{:S(2)}, u32[]{:S(2)}) %all-to-all-start.1) | async-done | bytes 8388640 | tf_op jit(solution)/shard_map/all_to_all | solution.py:152
  598.5 12.1 %copy.63 = bf16[1,64,8,4,2048]{4,3,2,1,0:T(4,128)(2,1)} copy(bf16[1,64,8,4,2048]{4,1,3,2,0:T(8,128)(2,1)} %bitcast.27) | data formatting | bytes 16777216 | tf_op jit(solution)/shard_map/all_to_all | solution.py:152
  610.6 12.5 %reshape.271 = bf16[2048,2048]{1,0:T(8,128)(2,1)} reshape(bf16[1,64,8,4,2048]{4,3,2,1,0:T(4,128)(2,1)} %copy.63) | data formatting | bytes 16777216 | tf_op jit(solution)/shard_map/reshape | solution.py:153
  623.1 13.4 %gather_fusion.1 = bf16[1024,2048]{1,0:T(8,128)(2,1)} fusion(bf16[2048,2048]{1,0:T(8,128)(2,1)} %reshape.271, s32[1024]{0:T(1024)S(1)} %broadcast_clamp_fusion), kind=kCustom, calls=%fused_computation.1 | custom fusion | bytes 8392704 | tf_op jit(solution)/shard_map/jit(_take)/gather | solution.py:154
  636.5 7.6 %gather.15 = bf16[512,2,2048]{2,1,0:T(2,128)(2,1)} reshape(bf16[1024,2048]{1,0:T(8,128)(2,1)} %gather_fusion.1) | data formatting | bytes 8388608 | tf_op jit(solution)/shard_map/jit(_take)/gather | solution.py:154
  644.1 20.0 %multiply_reduce_fusion = bf16[512,2048]{1,0:T(8,128)(2,1)} fusion(bf16[512,2,2048]{2,1,0:T(2,128)(2,1)} %gather.15, pred[512,2]{1,0:T(8,128)(4,1)S(1)} %copy.57, f32[512,2]{1,0:T(8,128)S(1)} %copy.64), kind=kLoop, calls=%fused_computation.39 | loop fusion | flops 7340032 | bytes 6296576 | tf_op jit(solution)/shard_map/reduce_sum | solution.py:155
  (118 shorter events, 52.5 us)
Async XLA Ops:
  7.2 149.4 %copy-start = (bf16[256,2048]{1,0:T(8,128)(2,1)S(1)}, bf16[256,2048]{1,0:T(8,128)(2,1)}, u32[]{:S(2)}) copy-start(bf16[256,2048]{1,0:T(8,128)(2,1)} %param.19) | copy-start | bytes 3145732
  7.2 16.9 %copy-start.3 = (bf16[512,2048]{1,0:T(8,128)(2,1)S(1)}, bf16[512,2048]{1,0:T(8,128)(2,1)}, u32[]{:S(2)}) copy-start(bf16[512,2048]{1,0:T(8,128)(2,1)} %param.21) | copy-start | bytes 6291460
  7.2 17.4 %copy-start.15 = (f32[2048]{0:T(1024)S(1)}, f32[2048]{0:T(1024)}, u32[]{:S(2)}) copy-start(f32[2048]{0:T(1024)} %param.24) | copy-start | bytes 24580
  7.2 247.0 %all-gather.5.cloned.1.call-start = ((), (), s32[]{:S(2)}) async-start(), calls=%async_computation.5 | async-start | bytes 20971520 | tf_op jit(solution)/shard_map/all_gather | solution.py:114
  7.9 322.4 %all-gather.3.cloned.1.call-start = ((), (), s32[]{:S(2)}) async-start(), calls=%async_computation.4 | async-start | bytes 20971520 | tf_op jit(solution)/shard_map/all_gather | solution.py:113
  55.1 7.3 %copy-start.6 = (bf16[1024,64]{0,1:T(8,128)(2,1)S(1)}, bf16[1024,64]{0,1:T(8,128)(2,1)}, u32[]{:S(2)}) copy-start(bf16[1024,64]{0,1:T(8,128)(2,1)} %param.16) | copy-start | bytes 393220
  55.1 7.3 %copy-start.7 = (bf16[1024,64]{0,1:T(8,128)(2,1)S(1)}, bf16[1024,64]{0,1:T(8,128)(2,1)}, u32[]{:S(2)}) copy-start(bf16[1024,64]{0,1:T(8,128)(2,1)} %param.17) | copy-start | bytes 393220
  55.1 76.1 %copy-start.8 = (f32[4]{0:T(128)S(1)}, f32[4]{0:T(128)}, u32[]{:S(2)}) copy-start(f32[4]{0:T(128)} %param.18) | copy-start | bytes 52
  55.1 190.8 %all-to-all-start = ((bf16[1,64,32,2048]{3,1,0,2:T(8,128)(2,1)}), bf16[1,64,32,2048]{3,1,0,2:T(8,128)(2,1)}, u32[]{:S(2)}, u32[]{:S(2)}) async-start(bf16[1,64,32,2048]{3,1,0,2:T(8,128)(2,1)} %copy_select_fusion), calls=%async_computation.1 | async-start | bytes 16777216 | tf_op jit(solution)/shard_map/all_to_all | solution.py:110
  62.4 353.3 %reduce-scatter.2.cloned.1.call-start = ((), (), s32[]{:S(2)}) async-start(), calls=%async_computation.3 | async-start | bytes 10485760 | tf_op jit(solution)/shard_map/reduce_scatter | solution.py:84
  62.5 68.7 %collective-permute-start = (bf16[128,128]{0,1:T(8,128)(2,1)S(1)}, bf16[128,128]{0,1:T(8,128)(2,1)S(1)}, u32[]{:S(2)}, u32[]{:S(2)}) collective-permute-start(bf16[128,128]{0,1:T(8,128)(2,1)S(1)} %get-tuple-element.110), channel_id=1, source_target_pairs={{0,4},{4,8},{8,12},{12,16},{16,20},{20,24},{24,28},{1,5},{5,9},{9,... | collective-permute-start | bytes 98312 | tf_op jit(solution)/shard_map/ppermute | solution.py:20
  66.4 64.8 %collective-permute-start.1 = (bf16[128,128]{0,1:T(8,128)(2,1)S(1)}, bf16[128,128]{0,1:T(8,128)(2,1)S(1)}, u32[]{:S(2)}, u32[]{:S(2)}) collective-permute-start(bf16[128,128]{0,1:T(8,128)(2,1)S(1)} %get-tuple-element.111), channel_id=1, source_target_pairs={{4,0},{8,4},{12,8},{16,12},{20,16},{24,20},{28,24},{5,1},{9,5},{13... | collective-permute-start | bytes 98312 | tf_op jit(solution)/shard_map/ppermute | solution.py:23
  67.7 300.4 %collective-permute-start.2 = (bf16[4,2048,256]{2,1,0:T(8,128)(2,1)}, bf16[4,2048,256]{2,1,0:T(8,128)(2,1)}, u32[]{:S(2)}, u32[]{:S(2)}) collective-permute-start(bf16[4,2048,256]{2,1,0:T(8,128)(2,1)} %param.27), channel_id=1, source_target_pairs={{0,3},{1,0},{2,1},{3,2},{4,7},{5,4},{6,5},{7,6},{8,11},{9,8},{10,9... | collective-permute-start | bytes 12582920 | tf_op jit(solution)/shard_map/ppermute | solution.py:132
  67.8 164.1 %collective-permute-start.3 = (bf16[4,2048,256]{2,1,0:T(8,128)(2,1)}, bf16[4,2048,256]{2,1,0:T(8,128)(2,1)}, u32[]{:S(2)}, u32[]{:S(2)}) collective-permute-start(bf16[4,2048,256]{2,1,0:T(8,128)(2,1)} %param.27), channel_id=1, source_target_pairs={{0,1},{1,2},{2,3},{3,0},{4,5},{5,6},{6,7},{7,4},{8,9},{9,10},{10,1... | collective-permute-start | bytes 12582920 | tf_op jit(solution)/shard_map/ppermute | solution.py:130
  232.0 146.5 %collective-permute-start.4 = (bf16[4,2048,256]{2,1,0:T(8,128)(2,1)}, bf16[4,2048,256]{2,1,0:T(8,128)(2,1)}, u32[]{:S(2)}, u32[]{:S(2)}) collective-permute-start(bf16[4,2048,256]{2,1,0:T(8,128)(2,1)} %collective-permute-done.3), channel_id=1, source_target_pairs={{0,1},{1,2},{2,3},{3,0},{4,5},{5,6},{6,7},{7,4},{8,9},{9,10},{10,1... | collective-permute-start | bytes 12582920 | tf_op jit(solution)/shard_map/ppermute | solution.py:130
  330.4 18.6 %copy-start.5 = (bf16[4,2048,256]{2,1,0:T(8,128)(2,1)S(1)}, bf16[4,2048,256]{2,1,0:T(8,128)(2,1)}, u32[]{:S(2)}) copy-start(bf16[4,2048,256]{2,1,0:T(8,128)(2,1)} %param.27) | copy-start | bytes 12582916
  349.0 19.0 %copy-start.4 = (bf16[512,4,1024]{2,0,1:T(8,128)(2,1)}, bf16[512,4,1024]{2,0,1:T(8,128)(2,1)S(1)}, u32[]{:S(2)}) copy-start(bf16[512,4,1024]{2,0,1:T(8,128)(2,1)S(1)} %fusion.18) | copy-start | bytes 12582916
  409.3 5.6 copy-start.10
  409.3 5.9 copy-start.12
  409.3 6.1 copy-start.17
  409.3 6.3 copy-start.14
  409.3 8.2 %copy-start.16 = (f32[2048]{0:T(1024)S(1)}, f32[2048]{0:T(1024)}, u32[]{:S(2)}) copy-start(f32[2048]{0:T(1024)} %param.20) | copy-start | bytes 24580
  409.3 189.2 %all-to-all-start.1 = ((bf16[8,64,4,2048]{3,1,2,0:T(8,128)(2,1)}), bf16[8,64,4,2048]{3,1,2,0:T(8,128)(2,1)}, u32[]{:S(2)}, u32[]{:S(2)}) async-start(bf16[8,64,4,2048]{3,1,2,0:T(8,128)(2,1)} %copy.62), calls=%async_computation.2 | async-start | bytes 16777216 | tf_op jit(solution)/shard_map/all_to_all | solution.py:152
  623.1 41.0 %copy-start.1 = (bf16[256,2048]{1,0:T(8,128)(2,1)S(1)}, bf16[256,2048]{1,0:T(8,128)(2,1)}, u32[]{:S(2)}) copy-start(bf16[256,2048]{1,0:T(8,128)(2,1)} %param.19) | copy-start | bytes 3145732
  (5 other events, 11.6 us)
Sparse Core Ops, SparseCore 0:
  9.6 156.1 all-gather.4
  167.3 162.9 all-gather.2
  332.9 71.4 reduce-scatter.1
